TPU v7x, 32 devices: a whole 2x2x4 slice. The times are simulated.
32 devices in a mesh: kv: 8 (over z, y), tp: 4 (over x, core).
Axes of the slice: x: 2, y: 2, z: 4, core: 2. Of those that a mesh axis runs over, the one named last changes fastest.
Arguments:
- tokens: bfloat16 [16, 4096], P(None, ('kv', 'tp')), may hold values from -8 to 8
- gate_weights: bfloat16 [2, 4096, 11264], P(None, None, ('kv', 'tp')), may hold values from -0.09375 to 0.09375
- up_weights: bfloat16 [2, 4096, 11264], P(None, None, ('kv', 'tp')), may hold values from -0.09375 to 0.09375
- down_weights: bfloat16 [2, 11264, 4096], P(None, ('kv', 'tp')), may hold values from -0.4375 to 0.4375
- norm_gain: bfloat16 [3, 4096], P(None, ('kv', 'tp')), may hold values from 0.25 to 4.5
- norm_bias: bfloat16 [3, 4096], P(None, ('kv', 'tp')), may hold values from -3 to 3
- query_weight: bfloat16 [4096, 4096], P('kv', 'tp'), may hold values from -0.09375 to 0.09375
- forget_weight: bfloat16 [4096, 4096], P('kv', 'tp'), may hold values from -0.09375 to 0.09375
- input_weight: bfloat16 [4096, 4096], P('kv', 'tp'), may hold values from -0.09375 to 0.09375
- outgate_weight: bfloat16 [4096, 4096], P('kv', 'tp'), may hold values from -0.09375 to 0.09375
- lower_bound: float32 [4096], P('tp'), may hold values from 0.05 to 0.9
- head_gain: float32 [4096], P('tp'), may hold values from 0.1 to 1.9
- out_weight: bfloat16 [4096, 4096], P('tp'), may hold values from -0.25 to 0.25
- state: float32 [16, 32, 128, 128], P('kv', 'tp'), may hold values from -3 to 3
Outputs:
- mixed: bfloat16 [16, 4096], P(None, ('kv', 'tp'))
- new_state: float32 [16, 32, 128, 128], P('kv', 'tp')
All inputs are finite; a program needn't handle non-finite values.
Results may differ from a plain program's by a relative error of at most 0.022.
Values may be sent and summed in bfloat16 or wider, within the bound.
A program may use at most 64 MiB of HBM per device.

v0:
```python
import functools

import jax
import jax.numpy as jnp
from jax import lax
from jax.experimental import pallas as pl
from jax.experimental.pallas import tpu as pltpu
from jax.sharding import PartitionSpec as P

MESH = pl.DeviceIdType.MESH

HEAD = 128


residual_scale = 8.0**0.25
norm_eps = 1e-05
head_eps = 1e-06


def whole_norm(stream, gain_row, bias_row):
    row_mean = jnp.mean(stream, axis=-1, keepdims=True)
    centred = stream - row_mean
    spread = jnp.mean(centred * centred, axis=-1, keepdims=True)
    return centred * lax.rsqrt(spread + norm_eps) * gain_row.astype(jnp.float32) + bias_row.astype(
        jnp.float32
    )


def ffn_partial(whole_rows, gate_w, up_w, down_w):
    gate_proj = jnp.dot(whole_rows, gate_w, preferred_element_type=jnp.float32)
    up_proj = jnp.dot(whole_rows, up_w, preferred_element_type=jnp.float32)
    hidden = (jax.nn.silu(gate_proj) * up_proj).astype(jnp.bfloat16)
    return jnp.dot(hidden, down_w, preferred_element_type=jnp.float32)


def local(
    tokens,
    gate_weights,
    up_weights,
    down_weights,
    norm_gain,
    norm_bias,
    query_weight,
    forget_weight,
    input_weight,
    outgate_weight,
    lower_bound,
    head_gain,
    out_weight,
    state,
):
    own_cols = tokens.shape[1]
    col_offset = lax.axis_index(("kv", "tp")) * own_cols
    whole_tokens, whole_gain, whole_bias = (
        lax.all_gather(tokens, ("kv", "tp"), axis=1, tiled=True),
        lax.all_gather(norm_gain, ("kv", "tp"), axis=1, tiled=True),
        lax.all_gather(norm_bias, ("kv", "tp"), axis=1, tiled=True),
    )

    def finish(partial_value, residual_whole, index, want_whole):
        total = lax.psum(partial_value, ("kv", "tp"))
        stream = residual_scale * residual_whole + 0.5 * total
        normed = whole_norm(stream, whole_gain[index], whole_bias[index]).astype(jnp.bfloat16)
        if want_whole:
            return normed
        return lax.dynamic_slice_in_dim(normed, col_offset, own_cols, 1)

    partial_one = ffn_partial(whole_tokens, gate_weights[0], up_weights[0], down_weights[0])
    normed_one = finish(partial_one, whole_tokens.astype(jnp.float32), 0, True)
    seq_count = state.shape[0]
    head_count = state.shape[1]
    head_cols = query_weight.shape[1]
    weight_rows = query_weight.shape[0]
    seq_offset = lax.axis_index("kv") * seq_count
    block_rows = lax.dynamic_slice_in_dim(
        normed_one, lax.axis_index("kv") * weight_rows, weight_rows, 1
    )
    weights = (query_weight, forget_weight, input_weight, outgate_weight)
    projected = lax.psum_scatter(
        jnp.concatenate(
            [jnp.dot(block_rows, weight, preferred_element_type=jnp.float32) for weight in weights],
            axis=1,
        ).astype(jnp.bfloat16),
        "kv",
        scatter_dimension=0,
        tiled=True,
    )
    query_pre = projected[:, :head_cols].astype(jnp.float32).reshape(seq_count, head_count, HEAD)
    forget_pre = (
        projected[:, head_cols : 2 * head_cols]
        .astype(jnp.float32)
        .reshape(seq_count, head_count, HEAD)
    )
    input_pre = (
        projected[:, 2 * head_cols : 3 * head_cols]
        .astype(jnp.float32)
        .reshape(seq_count, head_count, HEAD)
    )
    outgate_pre = projected[:, 3 * head_cols :].astype(jnp.float32)
    low_bound = lower_bound.reshape(head_count, HEAD)
    forget = low_bound + (1.0 - low_bound) * jax.nn.sigmoid(forget_pre)
    key_part = (1.0 - low_bound) * jax.nn.sigmoid(-forget_pre)
    updated = forget[..., None] * state + key_part[..., None] * input_pre[:, :, None, :]
    readout = jnp.einsum(
        "shd,shde->she", jax.nn.silu(query_pre), updated, precision=lax.Precision.HIGHEST
    )
    readout = readout * lax.rsqrt(jnp.mean(readout * readout, axis=-1, keepdims=True) + head_eps)
    gated_out = (
        readout.reshape(seq_count, head_cols) * head_gain * jax.nn.silu(outgate_pre)
    ).astype(jnp.bfloat16)
    mixer_part = jnp.dot(gated_out, out_weight, preferred_element_type=jnp.float32)
    head_sum = lax.psum_scatter(
        mixer_part.astype(jnp.bfloat16), "tp", scatter_dimension=1, tiled=True
    ).astype(jnp.float32)
    piece_cols = head_sum.shape[1]
    own_normed = lax.dynamic_slice_in_dim(normed_one, seq_offset, seq_count, 0)
    own_normed = lax.dynamic_slice_in_dim(
        own_normed, lax.axis_index("tp") * piece_cols, piece_cols, 1
    )
    stream_own = (residual_scale * own_normed.astype(jnp.float32) + head_sum).astype(jnp.bfloat16)
    seq_rows = lax.all_gather(stream_own, "tp", axis=1, tiled=True)
    stream_two = lax.all_gather(seq_rows, "kv", axis=0, tiled=True)
    normed_two = whole_norm(stream_two.astype(jnp.float32), whole_gain[1], whole_bias[1]).astype(
        jnp.bfloat16
    )
    partial_two = ffn_partial(normed_two, gate_weights[1], up_weights[1], down_weights[1])
    mixed = finish(partial_two, normed_two.astype(jnp.float32), 2, False)
    return (mixed, updated)


TOK, GB, RS_ONE, AG_ONE, RS_KV, RS_TP, AG_TWO, RS_THREE, AG_THREE = range(9)
PHASES = 9


def tree_sum(terms):
    while len(terms) > 1:
        rest = [terms[-1]] if len(terms) % 2 else []
        terms = [a + b for a, b in zip(terms[::2], terms[1::2])] + rest
    return terms[0]


def dot_turned(rows, weights):
    return lax.dot_general(
        rows, weights, (((1,), (1,)), ((), ())), preferred_element_type=jnp.float32
    )


def layer_kernel(
    n_kv,
    n_tp,
    tokens_ref,
    gain_ref,
    bias_ref,
    low_ref,
    head_gain_ref,
    gate_hbm,
    up_hbm,
    down_hbm,
    query_hbm,
    forget_hbm,
    input_hbm,
    outgate_hbm,
    out_hbm,
    state_hbm,
    mixed_ref,
    state_out,
    gate_v,
    up_v,
    down_v,
    proj_v,
    out_v,
    state_v,
    new_v,
    tok_buf,
    gb_own,
    gb_buf,
    rs_send,
    rs_recv_one,
    rs_recv_three,
    own_ag,
    ag_one,
    normed_f32,
    normed_bf,
    proj_f32,
    proj_send,
    proj_recv,
    gated_buf,
    tp_f32,
    tp_send,
    tp_recv,
    own_ag_two,
    ag_two,
    ag_two_f32,
    own_ag_three,
    ag_three,
    final_buf,
    send_sem,
    recv_sem,
    load_sem,
    store_sem,
):
    n = n_kv * n_tp
    batch, lane = tokens_ref.shape
    width = n * lane
    seqs, heads = state_v.shape[0], state_v.shape[1]
    kv, tp = lax.axis_index("kv"), lax.axis_index("tp")
    me = kv * n_tp + tp

    proj_hbm = (query_hbm, forget_hbm, input_hbm, outgate_hbm)
    loads = {}
    order = [("gate0", gate_hbm.at[0], gate_v.at[0]), ("up0", up_hbm.at[0], up_v.at[0])]
    order += [("down0", down_hbm.at[0], down_v.at[0])]
    order += [("proj%d" % i, proj_hbm[i], proj_v.at[i]) for i in range(4)]
    order += [("state", state_hbm, state_v), ("out", out_hbm, out_v)]
    order += [("gate1", gate_hbm.at[1], gate_v.at[1]), ("up1", up_hbm.at[1], up_v.at[1])]
    order += [("down1", down_hbm.at[1], down_v.at[1])]
    for i, (name, source, target) in enumerate(order):
        loads[name] = pltpu.make_async_copy(source, target, load_sem.at[i])
        loads[name].start()

    def peer_id(k):
        peer = lax.rem(me + k, n)
        return peer, (lax.div(peer, n_tp), lax.rem(peer, n_tp))

    barrier = pltpu.get_barrier_semaphore()

    @pl.loop(1, n)
    def _(k):
        _, device = peer_id(k)
        pl.semaphore_signal(barrier, inc=1, device_id=device, device_id_type=MESH)

    def slot(ref, index, rows):
        return ref.at[pl.ds(pl.multiple_of(index * rows, rows), rows)]

    def send_all(phase, src_of, dst, count, device_of):
        @pl.loop(1, count)
        def _(k):
            index, device = device_of(k)
            pltpu.make_async_remote_copy(
                src_ref=src_of(index),
                dst_ref=dst,
                send_sem=send_sem.at[phase],
                recv_sem=recv_sem.at[phase],
                device_id=device,
                device_id_type=MESH,
            ).start()

    def wait_bytes(sem, ref, rows):
        part = ref.at[pl.ds(0, rows)]
        pltpu.make_async_copy(part, part, sem).wait()

    gb_own[...] = jnp.zeros(gb_own.shape, jnp.float32)
    gb_own[0:3, :] = gain_ref[...].astype(jnp.float32)
    gb_own[3:6, :] = bias_ref[...].astype(jnp.float32)
    slot(gb_buf, me, 8)[...] = gb_own[...]
    slot(tok_buf, me, batch)[...] = tokens_ref[...]

    pl.semaphore_wait(barrier, n - 1)
    send_all(TOK, lambda i: tokens_ref, slot(tok_buf, me, batch), n, peer_id)
    send_all(GB, lambda i: gb_own, slot(gb_buf, me, 8), n, peer_id)

    def tiles_of(ref):
        return [ref[j * batch : (j + 1) * batch, :].astype(jnp.float32) for j in range(n)]

    def stats(tiles):
        mean = jnp.sum(tree_sum(tiles), axis=1, keepdims=True) / width
        centred = [tile - mean for tile in tiles]
        spread = jnp.sum(tree_sum([c * c for c in centred]), axis=1, keepdims=True) / width
        return mean, centred, lax.rsqrt(spread + norm_eps)

    def norm_tiles(tiles, index):
        _, centred, scale = stats(tiles)
        return [
            c * scale * gb_buf[8 * j + index : 8 * j + index + 1, :]
            + gb_buf[8 * j + 3 + index : 8 * j + 4 + index, :]
            for j, c in enumerate(centred)
        ]

    def ffn(rows, layer):
        step = 4 * lane
        gate = jnp.zeros((batch, gate_v.shape[1]), jnp.float32)
        up = jnp.zeros((batch, gate_v.shape[1]), jnp.float32)
        loads["gate%d" % layer].wait()
        loads["up%d" % layer].wait()
        for k in range(0, width, step):
            piece = rows[:, k : k + step]
            gate += dot_turned(piece, gate_v[layer, :, k : k + step])
            up += dot_turned(piece, up_v[layer, :, k : k + step])
        hidden = (jax.nn.silu(gate) * up).astype(jnp.bfloat16)
        loads["down%d" % layer].wait()
        for k in range(0, width, step):
            part = jnp.dot(
                hidden, down_v[layer, :, k : k + step], preferred_element_type=jnp.float32
            ).astype(jnp.bfloat16)
            for j in range(step // lane):
                first = (k // lane + j) * batch
                rs_send[first : first + batch, :] = part[:, j * lane : (j + 1) * lane]

    def reduce_scatter(phase, recv):
        send_all(phase, lambda i: slot(rs_send, i, batch), slot(recv, me, batch), n, peer_id)
        slot(recv, me, batch)[...] = slot(rs_send, me, batch)[...]
        wait_bytes(recv_sem.at[phase], recv, (n - 1) * batch)
        return tree_sum(tiles_of(recv))

    wait_bytes(recv_sem.at[TOK], tok_buf, (n - 1) * batch)
    ffn(jnp.concatenate([tok_buf[j * batch : (j + 1) * batch, :] for j in range(n)], axis=1), 0)
    total = reduce_scatter(RS_ONE, rs_recv_one)
    stream = residual_scale * tokens_ref[...].astype(jnp.float32) + 0.5 * total
    own_ag[...] = stream.astype(jnp.bfloat16)
    slot(ag_one, me, batch)[...] = stream.astype(jnp.bfloat16)
    send_all(AG_ONE, lambda i: own_ag, slot(ag_one, me, batch), n, peer_id)
    wait_bytes(recv_sem.at[GB], gb_buf, (n - 1) * 8)
    wait_bytes(recv_sem.at[AG_ONE], ag_one, (n - 1) * batch)
    for j, tile in enumerate(norm_tiles(tiles_of(ag_one), 0)):
        rounded = tile.astype(jnp.bfloat16)
        normed_bf[j * batch : (j + 1) * batch, :] = rounded
        normed_f32[j * batch : (j + 1) * batch, :] = rounded.astype(jnp.float32)

    own_rows = slot(normed_bf, kv, n_tp * batch)
    block = jnp.concatenate(
        [own_rows[j * batch : (j + 1) * batch, :] for j in range(n_tp)], axis=1
    )
    per_seq = 4 * heads
    for i in range(4):
        loads["proj%d" % i].wait()
        part = jnp.dot(block, proj_v[i], preferred_element_type=jnp.float32)
        for h in range(heads):
            for r in range(0, batch, 8):
                proj_f32[pl.ds(r * per_seq + i * heads + h, 8, stride=per_seq), :] = part[
                    r : r + 8, h * HEAD : (h + 1) * HEAD
                ]
    proj_send[...] = proj_f32[...].astype(jnp.bfloat16)
    block_len = seqs * per_seq

    def kv_peer(k):
        peer = lax.rem(kv + k, n_kv)
        return peer, (peer, tp)

    send_all(
        RS_KV,
        lambda i: slot(proj_send, i, block_len),
        slot(proj_recv, kv, block_len),
        n_kv,
        kv_peer,
    )
    slot(proj_recv, kv, block_len)[...] = slot(proj_send, kv, block_len)[...]
    wait_bytes(recv_sem.at[RS_KV], proj_recv, (n_kv - 1) * block_len)
    projected = tree_sum(
        [
            proj_recv[j * block_len : (j + 1) * block_len, :].astype(jnp.float32)
            for j in range(n_kv)
        ]
    )
    projected = projected.astype(jnp.bfloat16).astype(jnp.float32)

    low = low_ref[...]
    loads["state"].wait()
    for s in range(seqs):
        base = s * per_seq
        query_pre = projected[base : base + heads]
        forget_pre = projected[base + heads : base + 2 * heads]
        input_pre = projected[base + 2 * heads : base + 3 * heads]
        outgate_pre = projected[base + 3 * heads : base + 4 * heads]
        forget = low + (1.0 - low) * jax.nn.sigmoid(forget_pre)
        key_part = (1.0 - low) * jax.nn.sigmoid(-forget_pre)
        fill = jnp.zeros((HEAD - 3 * heads, HEAD), jnp.float32)
        turned = jnp.concatenate([forget, key_part, jax.nn.silu(query_pre), fill], axis=0).T
        readouts = []
        for h in range(heads):
            updated = (
                turned[:, h : h + 1] * state_v[s, h]
                + turned[:, heads + h : heads + h + 1] * input_pre[h : h + 1, :]
            )
            new_v[s, h] = updated
            query_col = turned[:, 2 * heads + h : 2 * heads + h + 1]
            readouts.append(jnp.sum(query_col * updated, axis=0, keepdims=True))
        readout = jnp.concatenate(readouts, axis=0)
        mean_square = jnp.mean(readout * readout, axis=1, keepdims=True)
        readout = readout * lax.rsqrt(mean_square + head_eps)
        gated_buf[s * heads : (s + 1) * heads, :] = (
            readout * head_gain_ref[...] * jax.nn.silu(outgate_pre)
        )
    store = pltpu.make_async_copy(new_v, state_out, store_sem)
    store.start()

    gated = jnp.concatenate(
        [gated_buf[pl.ds(h, seqs, stride=heads), :] for h in range(heads)], axis=1
    ).astype(jnp.bfloat16)
    loads["out"].wait()
    step = 4 * lane
    rows_tp = seqs * heads
    for k in range(0, width, step):
        part = jnp.dot(gated, out_v[:, k : k + step], preferred_element_type=jnp.float32)
        for j in range(step // lane):
            tile = k // lane + j
            first = (tile // heads) * rows_tp + tile % heads
            tp_f32[pl.ds(first, seqs, stride=heads), :] = part[:, j * lane : (j + 1) * lane]
    tp_send[...] = tp_f32[...].astype(jnp.bfloat16)

    def tp_peer(k):
        peer = lax.rem(tp + k, n_tp)
        return peer, (kv, peer)

    send_all(
        RS_TP, lambda i: slot(tp_send, i, rows_tp), slot(tp_recv, tp, rows_tp), n_tp, tp_peer
    )
    slot(tp_recv, tp, rows_tp)[...] = slot(tp_send, tp, rows_tp)[...]
    residual = jnp.concatenate(
        [
            normed_f32[pl.ds(tp * (heads * batch) + kv * seqs + s, heads, stride=batch), :]
            for s in range(seqs)
        ],
        axis=0,
    )
    wait_bytes(recv_sem.at[RS_TP], tp_recv, (n_tp - 1) * rows_tp)
    head_sum = tree_sum(
        [tp_recv[j * rows_tp : (j + 1) * rows_tp, :].astype(jnp.float32) for j in range(n_tp)]
    )
    stream_two = (residual_scale * residual + head_sum).astype(jnp.bfloat16)
    own_ag_two[...] = stream_two
    slot(ag_two, me, rows_tp)[...] = stream_two
    send_all(AG_TWO, lambda i: own_ag_two, slot(ag_two, me, rows_tp), n, peer_id)
    wait_bytes(recv_sem.at[AG_TWO], ag_two, (n - 1) * rows_tp)
    ag_two_f32[...] = ag_two[...].astype(jnp.float32)
    tiles = [
        jnp.concatenate(
            [
                ag_two_f32[
                    pl.ds((j // heads) * rows_tp + s * heads + j % heads, n_kv, stride=n_tp * rows_tp),
                    :,
                ]
                for s in range(seqs)
            ],
            axis=0,
        )
        for j in range(n)
    ]
    normed = [tile.astype(jnp.bfloat16) for tile in norm_tiles(tiles, 1)]
    wait_bytes(send_sem.at[RS_ONE], rs_recv_one, (n - 1) * batch)
    for j, tile in enumerate(normed):
        normed_bf[j * batch : (j + 1) * batch, :] = tile
    ffn(jnp.concatenate(normed, axis=1), 1)
    total = reduce_scatter(RS_THREE, rs_recv_three)
    residual = slot(normed_bf, me, batch)[...].astype(jnp.float32)
    stream = residual_scale * residual + 0.5 * total
    own_ag_three[...] = stream.astype(jnp.bfloat16)
    slot(ag_three, me, batch)[...] = stream.astype(jnp.bfloat16)
    send_all(AG_THREE, lambda i: own_ag_three, slot(ag_three, me, batch), n, peer_id)
    wait_bytes(recv_sem.at[AG_THREE], ag_three, (n - 1) * batch)
    mean, _, scale = stats(tiles_of(ag_three))
    mixed = (stream - mean) * scale * gb_own[2:3, :] + gb_own[5:6, :]
    for s in range(seqs):
        final_buf[pl.ds(s, n_kv, stride=seqs), :] = mixed[s * n_kv : (s + 1) * n_kv, :]
    mixed_ref[...] = final_buf[...].astype(jnp.bfloat16)

    for phase in (TOK, AG_ONE, AG_TWO, RS_THREE, AG_THREE):
        wait_bytes(send_sem.at[phase], tok_buf, (n - 1) * batch)
    wait_bytes(send_sem.at[GB], gb_buf, (n - 1) * 8)
    wait_bytes(send_sem.at[RS_KV], proj_recv, (n_kv - 1) * block_len)
    wait_bytes(send_sem.at[RS_TP], tp_recv, (n_tp - 1) * rows_tp)
    store.wait()


def fused(n_kv, n_tp, *args):
    (
        tokens,
        gate_weights,
        up_weights,
        down_weights,
        norm_gain,
        norm_bias,
        query_weight,
        forget_weight,
        input_weight,
        outgate_weight,
        lower_bound,
        head_gain,
        out_weight,
        state,
    ) = args
    batch, lane = tokens.shape
    n = n_kv * n_tp
    seqs, heads = state.shape[:2]
    gate_weights = jnp.swapaxes(gate_weights, 1, 2)
    up_weights = jnp.swapaxes(up_weights, 1, 2)
    bf16, f32 = jnp.bfloat16, jnp.float32
    per_seq = 4 * heads
    rows_tp = seqs * heads
    scratch = [
        pltpu.VMEM(gate_weights.shape, bf16),
        pltpu.VMEM(up_weights.shape, bf16),
        pltpu.VMEM(down_weights.shape, bf16),
        pltpu.VMEM((4, *query_weight.shape), bf16),
        pltpu.VMEM(out_weight.shape, bf16),
        pltpu.VMEM(state.shape, f32),
        pltpu.VMEM(state.shape, f32),
        pltpu.VMEM((n * batch, lane), bf16),
        pltpu.VMEM((8, lane), f32),
        pltpu.VMEM((n * 8, lane), f32),
        pltpu.VMEM((n * batch, lane), bf16),
        pltpu.VMEM((n * batch, lane), bf16),
        pltpu.VMEM((n * batch, lane), bf16),
        pltpu.VMEM((batch, lane), bf16),
        pltpu.VMEM((n * batch, lane), bf16),
        pltpu.VMEM((n * batch, lane), f32),
        pltpu.VMEM((n * batch, lane), bf16),
        pltpu.VMEM((batch * per_seq, HEAD), f32),
        pltpu.VMEM((batch * per_seq, HEAD), bf16),
        pltpu.VMEM((batch * per_seq, HEAD), bf16),
        pltpu.VMEM((rows_tp, HEAD), f32),
        pltpu.VMEM((n_tp * rows_tp, HEAD), f32),
        pltpu.VMEM((n_tp * rows_tp, HEAD), bf16),
        pltpu.VMEM((n_tp * rows_tp, HEAD), bf16),
        pltpu.VMEM((rows_tp, HEAD), bf16),
        pltpu.VMEM((n * rows_tp, HEAD), bf16),
        pltpu.VMEM((n * rows_tp, HEAD), f32),
        pltpu.VMEM((batch, lane), bf16),
        pltpu.VMEM((n * batch, lane), bf16),
        pltpu.VMEM((batch, lane), f32),
        pltpu.SemaphoreType.DMA((PHASES,)),
        pltpu.SemaphoreType.DMA((PHASES,)),
        pltpu.SemaphoreType.DMA((12,)),
        pltpu.SemaphoreType.DMA,
    ]
    vmem = pl.BlockSpec(memory_space=pltpu.VMEM)
    hbm = pl.BlockSpec(memory_space=pl.ANY)
    return pl.pallas_call(
        functools.partial(layer_kernel, n_kv, n_tp),
        out_shape=(
            jax.ShapeDtypeStruct(tokens.shape, bf16),
            jax.ShapeDtypeStruct(state.shape, f32),
        ),
        in_specs=[vmem] * 5 + [hbm] * 9,
        out_specs=(vmem, hbm),
        scratch_shapes=scratch,
        compiler_params=pltpu.CompilerParams(
            collective_id=0, has_side_effects=True, vmem_limit_bytes=60 * 1024 * 1024
        ),
        name="layer",
    )(
        tokens,
        norm_gain,
        norm_bias,
        lower_bound.reshape(heads, HEAD),
        head_gain.reshape(heads, HEAD),
        gate_weights,
        up_weights,
        down_weights,
        query_weight,
        forget_weight,
        input_weight,
        outgate_weight,
        out_weight,
        state,
    )


def dispatch(n_kv, n_tp, *args):
    tokens, state = args[0], args[13]
    batch, lane = tokens.shape
    whole_tiles = lane == HEAD and batch % 16 == 0 and (state.shape[0] * state.shape[1]) % 16 == 0
    if whole_tiles and state.shape[1] == 8 and n_kv % 8 == 0:
        return fused(n_kv, n_tp, *args)
    return local(*args)


def solution(mesh):
    n_kv, n_tp = mesh.shape["kv"], mesh.shape["tp"]
    return jax.shard_map(
        functools.partial(dispatch, n_kv, n_tp),
        mesh=mesh,
        in_specs=(
            P(None, ("kv", "tp")),
            P(None, None, ("kv", "tp")),
            P(None, None, ("kv", "tp")),
            P(None, ("kv", "tp"), None),
            P(None, ("kv", "tp")),
            P(None, ("kv", "tp")),
            P("kv", "tp"),
            P("kv", "tp"),
            P("kv", "tp"),
            P("kv", "tp"),
            P("tp"),
            P("tp"),
            P("tp", None),
            P("kv", "tp", None, None),
        ),
        out_specs=(P(None, ("kv", "tp")), P("kv", "tp", None, None)),
        check_vma=False,
    )
```

profile of v0, /device:TPU:0, one launch (start us, length us, event | category | flops | bytes accessed | tf_op | source)
XLA Modules:
  0.0 62.7 jit_solution(1397103277918815861)
XLA Ops:
  0.6 58.5 %layer.1 = (bf16[16,128]{1,0:T(8,128)(2,1)}, f32[2,8,128,128]{3,2,1,0:T(8,128)}) custom-call(bf16[16,128]{1,0:T(8,128)(2,1)} %tokens_ref.1, bf16[3,128]{1,0:T(4,128)(2,1)} %gain_ref.1, bf16[3,128]{1,0:T(4,128)(2,1)} %bias_ref.1, f32[8,128]{1,0:T(8,128)} %bitcast.6, f32[8,128]{1,0:T(8,128)} %bitcast.7, bf16[2,352,4096]{2,1,0:T(8,128)(2,1)} %bitcast.4, ...), custom_call_target="tpu_custom_call" | custom-call | tf_op jit(solution)/shard_map/layer/pallas_call | solution.py:527
  59.1 1.3 %copy.18 = bf16[16,128]{1,0:T(8,128)(2,1)} copy(bf16[16,128]{1,0:T(8,128)(2,1)} %get-tuple-element.4) | data formatting | bytes 8192
  60.4 2.3 %copy.19 = f32[2,8,128,128]{3,2,1,0:T(8,128)} copy(f32[2,8,128,128]{3,2,1,0:T(8,128)} %get-tuple-element.5) | data formatting | bytes 2097152
where the time goes:
time: 62.9 us; the launch traced here: 62.7 us
  Pallas kernels  58.5 us (93%)
  local copies, waits for them, and re-layouts  3.57 us (6%)
  between operations  0.64 us (1%)
    pallas_call x1, Pallas kernels, fused(): pl.pallas_call(functools.partial(layer_kernel, n_kv, n_tp), out_shape=(ja...  58.5 us
    unnamed x2, local copies, waits for them, and re-layouts  3.57 us

commit v1 on v0

v1 whole, which is shorter than its diff:
```python
import functools

import jax
import jax.numpy as jnp
from jax import lax
from jax.experimental import pallas as pl
from jax.experimental.pallas import tpu as pltpu
from jax.sharding import PartitionSpec as P

MESH = pl.DeviceIdType.MESH

HEAD = 128


residual_scale = 8.0**0.25
norm_eps = 1e-05
head_eps = 1e-06


def whole_norm(stream, gain_row, bias_row):
    row_mean = jnp.mean(stream, axis=-1, keepdims=True)
    centred = stream - row_mean
    spread = jnp.mean(centred * centred, axis=-1, keepdims=True)
    return centred * lax.rsqrt(spread + norm_eps) * gain_row.astype(jnp.float32) + bias_row.astype(
        jnp.float32
    )


def ffn_partial(whole_rows, gate_w, up_w, down_w):
    gate_proj = jnp.dot(whole_rows, gate_w, preferred_element_type=jnp.float32)
    up_proj = jnp.dot(whole_rows, up_w, preferred_element_type=jnp.float32)
    hidden = (jax.nn.silu(gate_proj) * up_proj).astype(jnp.bfloat16)
    return jnp.dot(hidden, down_w, preferred_element_type=jnp.float32)


def local(
    tokens,
    gate_weights,
    up_weights,
    down_weights,
    norm_gain,
    norm_bias,
    query_weight,
    forget_weight,
    input_weight,
    outgate_weight,
    lower_bound,
    head_gain,
    out_weight,
    state,
):
    own_cols = tokens.shape[1]
    col_offset = lax.axis_index(("kv", "tp")) * own_cols
    whole_tokens, whole_gain, whole_bias = (
        lax.all_gather(tokens, ("kv", "tp"), axis=1, tiled=True),
        lax.all_gather(norm_gain, ("kv", "tp"), axis=1, tiled=True),
        lax.all_gather(norm_bias, ("kv", "tp"), axis=1, tiled=True),
    )

    def finish(partial_value, residual_whole, index, want_whole):
        total = lax.psum(partial_value, ("kv", "tp"))
        stream = residual_scale * residual_whole + 0.5 * total
        normed = whole_norm(stream, whole_gain[index], whole_bias[index]).astype(jnp.bfloat16)
        if want_whole:
            return normed
        return lax.dynamic_slice_in_dim(normed, col_offset, own_cols, 1)

    partial_one = ffn_partial(whole_tokens, gate_weights[0], up_weights[0], down_weights[0])
    normed_one = finish(partial_one, whole_tokens.astype(jnp.float32), 0, True)
    seq_count = state.shape[0]
    head_count = state.shape[1]
    head_cols = query_weight.shape[1]
    weight_rows = query_weight.shape[0]
    seq_offset = lax.axis_index("kv") * seq_count
    block_rows = lax.dynamic_slice_in_dim(
        normed_one, lax.axis_index("kv") * weight_rows, weight_rows, 1
    )
    weights = (query_weight, forget_weight, input_weight, outgate_weight)
    projected = lax.psum_scatter(
        jnp.concatenate(
            [jnp.dot(block_rows, weight, preferred_element_type=jnp.float32) for weight in weights],
            axis=1,
        ).astype(jnp.bfloat16),
        "kv",
        scatter_dimension=0,
        tiled=True,
    )
    query_pre = projected[:, :head_cols].astype(jnp.float32).reshape(seq_count, head_count, HEAD)
    forget_pre = (
        projected[:, head_cols : 2 * head_cols]
        .astype(jnp.float32)
        .reshape(seq_count, head_count, HEAD)
    )
    input_pre = (
        projected[:, 2 * head_cols : 3 * head_cols]
        .astype(jnp.float32)
        .reshape(seq_count, head_count, HEAD)
    )
    outgate_pre = projected[:, 3 * head_cols :].astype(jnp.float32)
    low_bound = lower_bound.reshape(head_count, HEAD)
    forget = low_bound + (1.0 - low_bound) * jax.nn.sigmoid(forget_pre)
    key_part = (1.0 - low_bound) * jax.nn.sigmoid(-forget_pre)
    updated = forget[..., None] * state + key_part[..., None] * input_pre[:, :, None, :]
    readout = jnp.einsum(
        "shd,shde->she", jax.nn.silu(query_pre), updated, precision=lax.Precision.HIGHEST
    )
    readout = readout * lax.rsqrt(jnp.mean(readout * readout, axis=-1, keepdims=True) + head_eps)
    gated_out = (
        readout.reshape(seq_count, head_cols) * head_gain * jax.nn.silu(outgate_pre)
    ).astype(jnp.bfloat16)
    mixer_part = jnp.dot(gated_out, out_weight, preferred_element_type=jnp.float32)
    head_sum = lax.psum_scatter(
        mixer_part.astype(jnp.bfloat16), "tp", scatter_dimension=1, tiled=True
    ).astype(jnp.float32)
    piece_cols = head_sum.shape[1]
    own_normed = lax.dynamic_slice_in_dim(normed_one, seq_offset, seq_count, 0)
    own_normed = lax.dynamic_slice_in_dim(
        own_normed, lax.axis_index("tp") * piece_cols, piece_cols, 1
    )
    stream_own = (residual_scale * own_normed.astype(jnp.float32) + head_sum).astype(jnp.bfloat16)
    seq_rows = lax.all_gather(stream_own, "tp", axis=1, tiled=True)
    stream_two = lax.all_gather(seq_rows, "kv", axis=0, tiled=True)
    normed_two = whole_norm(stream_two.astype(jnp.float32), whole_gain[1], whole_bias[1]).astype(
        jnp.bfloat16
    )
    partial_two = ffn_partial(normed_two, gate_weights[1], up_weights[1], down_weights[1])
    mixed = finish(partial_two, normed_two.astype(jnp.float32), 2, False)
    return (mixed, updated)


KINDS = ("gb", "rs_one", "turn", "own_tp", "base", "rs_three", "spread")


def tree_sum(terms):
    while len(terms) > 1:
        rest = [terms[-1]] if len(terms) % 2 else []
        terms = [a + b for a, b in zip(terms[::2], terms[1::2])] + rest
    return terms[0]


def total_of(tiles):
    rows = jnp.sum(tree_sum(tiles), axis=0, keepdims=True)
    return jnp.sum(rows, axis=1, keepdims=True)


def dot_turned(rows, weights):
    return lax.dot_general(
        rows, weights, (((1,), (1,)), ((), ())), preferred_element_type=jnp.float32
    )


def flipped(value, count, mask):
    out, bit = value, 1
    while bit < count:
        if mask & bit:
            out = out + bit - 2 * bit * lax.rem(lax.div(value, bit), 2)
        bit *= 2
    return out


def layer_kernel(
    n_kv,
    n_tp,
    tokens_hbm,
    gain_hbm,
    bias_hbm,
    low_hbm,
    head_gain_hbm,
    gate_hbm,
    up_hbm,
    down_hbm,
    query_hbm,
    forget_hbm,
    input_hbm,
    outgate_hbm,
    out_hbm,
    state_hbm,
    mixed_ref,
    state_out,
    gate_v,
    up_v,
    down_v,
    proj_v,
    out_v,
    state_v,
    new_v,
    gain_v,
    bias_v,
    low_v,
    head_gain_v,
    tok_buf,
    gb_buf,
    rs_send,
    rs_recv_one,
    rs_recv_three,
    turn_send,
    turn_recv,
    own_tp,
    base_f32,
    base_send,
    base_recv,
    proj_f32,
    proj_send,
    proj_recv,
    gated_buf,
    head_f32,
    head_buf,
    ag_two,
    ag_two_f32,
    normed_bf,
    spread_buf,
    final_buf,
    send_sem,
    recv_sem,
    tok_sem,
    proj_sem,
    head_sem,
    ag_sem,
    load_sem,
    store_sem,
):
    n = n_kv * n_tp
    batch, lane = tok_buf.shape[1:]
    width = n * lane
    seqs, heads = state_v.shape[0], state_v.shape[1]
    part_rows = ag_two.shape[2]
    per = part_rows // seqs
    parts = n // per
    group = n_tp * lane
    bf16, f32 = jnp.bfloat16, jnp.float32
    kv, tp = lax.axis_index("kv"), lax.axis_index("tp")
    me = kv * n_tp + tp
    kv_of = [flipped(kv, n_kv, m) for m in range(n_kv)]
    tp_of = [flipped(tp, n_tp, m) for m in range(n_tp)]
    peers = [(k, t) for k in reversed(range(n_kv)) for t in reversed(range(n_tp)) if k or t]

    barrier = pltpu.get_barrier_semaphore()
    for k, t in peers:
        pl.semaphore_signal(
            barrier, inc=1, device_id=(kv_of[k], tp_of[t]), device_id_type=MESH
        )

    proj_hbm = (query_hbm, forget_hbm, input_hbm, outgate_hbm)
    loads = {}
    order = [("tokens", tokens_hbm, tok_buf.at[me])]
    order += [("gain", gain_hbm, gain_v), ("bias", bias_hbm, bias_v)]
    order += [("gate0", gate_hbm.at[0], gate_v.at[0]), ("up0", up_hbm.at[0], up_v.at[0])]
    order += [("down0", down_hbm.at[0], down_v.at[0])]
    order += [("proj%d" % i, proj_hbm[i], proj_v.at[i]) for i in range(4)]
    order += [("low", low_hbm, low_v), ("head_gain", head_gain_hbm, head_gain_v)]
    order += [("state", state_hbm, state_v), ("out", out_hbm, out_v)]
    order += [("gate1", gate_hbm.at[1], gate_v.at[1]), ("up1", up_hbm.at[1], up_v.at[1])]
    order += [("down1", down_hbm.at[1], down_v.at[1])]
    for i, (name, source, target) in enumerate(order):
        loads[name] = pltpu.make_async_copy(source, target, load_sem.at[i])
        loads[name].start()

    def send(src, dst, kind, recv, k, t):
        pltpu.make_async_remote_copy(
            src_ref=src,
            dst_ref=dst,
            send_sem=send_sem.at[kind],
            recv_sem=recv,
            device_id=(kv_of[k], tp_of[t]),
            device_id_type=MESH,
        ).start()

    def wait_for(sem, ref, count):
        part = ref.at[pl.ds(0, count)]
        pltpu.make_async_copy(part, part, sem).wait()

    GB, RS_ONE, TURN, OWN_TP, BASE, RS_THREE, SPREAD = range(len(KINDS))
    TOK, PROJ, HEADS_SUM, AG_TWO = range(len(KINDS), len(KINDS) + 4)

    loads["gain"].wait()
    loads["bias"].wait()
    pad = jnp.zeros((2, lane), f32)
    gains = jnp.concatenate([gain_v[...].astype(f32), bias_v[...].astype(f32), pad], axis=0)
    gb_buf[me] = gains
    loads["tokens"].wait()
    pl.semaphore_wait(barrier, n - 1)
    for k, t in peers:
        send(tok_buf.at[me], tok_buf.at[me], TOK, tok_sem.at[kv], k, t)
    for k, t in peers:
        send(gb_buf.at[me], gb_buf.at[me], GB, recv_sem.at[GB], k, t)

    def columns(index, size):
        return pl.ds(pl.multiple_of(index * size, size), size)

    def hidden_of(gate, up):
        return (jax.nn.silu(gate) * up).astype(bf16)

    def reduce_scatter_start(hidden, layer, kind, recv):
        loads["down%d" % layer].wait()
        for k in reversed(range(n_kv)):
            target = kv_of[k]
            part = jnp.dot(
                hidden, down_v[layer, :, columns(target, group)], preferred_element_type=f32
            ).astype(bf16)
            for t in range(n_tp):
                rs_send[target * n_tp + t] = part[:, t * lane : (t + 1) * lane]
            for t in reversed(range(n_tp)):
                if k or t:
                    index = target * n_tp + tp_of[t]
                    send(rs_send.at[index], recv.at[me], kind, recv_sem.at[kind], k, t)
        recv[me] = rs_send[me]

    def reduce_scatter_end(kind, recv):
        wait_for(recv_sem.at[kind], recv, n - 1)
        return tree_sum([recv[j].astype(f32) for j in range(n)])

    gate = up = None
    for k in range(n_kv):
        source = kv_of[k]
        wait_for(tok_sem.at[source], tok_buf, n_tp if k else n_tp - 1)
        rows = jnp.concatenate([tok_buf[source * n_tp + t] for t in range(n_tp)], axis=1)
        cols = columns(source, group)
        if k == 0:
            loads["gate0"].wait()
            loads["up0"].wait()
        gate_part = dot_turned(rows, gate_v[0, :, cols])
        up_part = dot_turned(rows, up_v[0, :, cols])
        gate = gate_part if gate is None else gate + gate_part
        up = up_part if up is None else up + up_part
    reduce_scatter_start(hidden_of(gate, up), 0, RS_ONE, rs_recv_one)

    token_sum = jnp.sum(
        tree_sum([tok_buf[j].astype(f32) for j in range(n)]), axis=1, keepdims=True
    )
    centre = residual_scale * token_sum / width
    own_tokens = residual_scale * tok_buf[me].astype(f32) - centre

    wait_for(recv_sem.at[GB], gb_buf, n - 1)
    kv_gains = jnp.concatenate([gb_buf[kv * n_tp + t] for t in range(n_tp)], axis=1).astype(bf16)
    for i in range(4):
        loads["proj%d" % i].wait()
        based = jnp.dot(kv_gains, proj_v[i], preferred_element_type=f32)
        for h in range(heads):
            block = slice(h * HEAD, (h + 1) * HEAD)
            base_f32[i, h : h + 1, :] = based[0:1, block]
            base_f32[i, heads + h : heads + h + 1, :] = based[3:4, block]
    base_send[...] = base_f32[...].astype(bf16)
    for k in reversed(range(1, n_kv)):
        send(base_send, base_recv.at[kv], BASE, recv_sem.at[BASE], k, 0)
    base_recv[kv] = base_send[...]

    shifted = own_tokens + 0.5 * reduce_scatter_end(RS_ONE, rs_recv_one)
    own_tp[tp] = (shifted * gains[0:1, :]).astype(bf16)
    for t in reversed(range(1, n_tp)):
        send(own_tp.at[tp], own_tp.at[tp], OWN_TP, recv_sem.at[OWN_TP], 0, t)
    for j in range(n_kv):
        turn_send[j] = shifted[j * seqs : (j + 1) * seqs, :]
    for k, t in peers:
        send(turn_send.at[kv_of[k]], turn_recv.at[me], TURN, recv_sem.at[TURN], k, t)
    turn_recv[me] = turn_send[kv]

    wait_for(recv_sem.at[OWN_TP], own_tp, n_tp - 1)
    block = jnp.concatenate([own_tp[t] for t in range(n_tp)], axis=1)
    turns = (1, 2, 0, 3)
    for i in turns:
        part = jnp.dot(block, proj_v[i], preferred_element_type=f32)
        for h in range(heads):
            for r in range(0, batch, 8):
                proj_f32[i, pl.ds(r * heads + h, 8, stride=heads), :] = part[
                    r : r + 8, h * HEAD : (h + 1) * HEAD
                ]
        proj_send[i] = proj_f32[i].reshape(proj_send.shape[1:]).astype(bf16)
        for k in reversed(range(1, n_kv)):
            send(proj_send.at[i, kv_of[k]], proj_recv.at[i, kv], PROJ, proj_sem.at[i], k, 0)
        proj_recv[i, kv] = proj_send[i, kv]

    wait_for(recv_sem.at[BASE], base_recv, n_kv - 1)
    base = tree_sum([base_recv[j].astype(f32) for j in range(n_kv)])
    wait_for(recv_sem.at[TURN], turn_recv, n - 1)

    def gain_rows(c, index):
        return gb_buf[c * per : (c + 1) * per, index, :]

    def norm_rows(tiles, index):
        mean = total_of(tiles) / width
        centred = [tile - mean for tile in tiles]
        scale = lax.rsqrt(total_of([c * c for c in centred]) / width + norm_eps)
        normed = [
            (tile * scale * gain_rows(c, index) + gain_rows(c, 3 + index)).astype(bf16)
            for c, tile in enumerate(centred)
        ]
        return mean, scale, normed

    norm_one = [
        norm_rows([turn_recv[c * per : (c + 1) * per, s, :] for c in range(parts)], 0)
        for s in range(seqs)
    ]
    residual = [
        [residual_scale * tile.astype(f32) for tile in norm_one[s][2]] for s in range(seqs)
    ]

    def projected(i):
        wait_for(proj_sem.at[i], proj_recv.at[i], n_kv - 1)
        total = tree_sum([proj_recv[i, j].astype(f32) for j in range(n_kv)])
        found = []
        for s in range(seqs):
            mean, scale, _ = norm_one[s]
            rows = total[s * heads : (s + 1) * heads] - mean * base[i, 0:heads]
            rows = scale * rows + base[i, heads : 2 * heads]
            found.append(rows.astype(bf16).astype(f32))
        return found

    loads["low"].wait()
    low = low_v[...]
    forget_pre = projected(1)
    forget = [low + (1.0 - low) * jax.nn.sigmoid(p) for p in forget_pre]
    key_part = [(1.0 - low) * jax.nn.sigmoid(-p) for p in forget_pre]
    input_pre = projected(2)
    query = [jax.nn.silu(p) for p in projected(0)]
    fill = jnp.zeros((HEAD - 3 * seqs * heads, HEAD), f32)
    seen = [q * f for q, f in zip(query, forget)]
    turned = jnp.concatenate([*seen, *forget, *key_part, fill], axis=0).T

    def column(kind, s, h):
        first = (kind * seqs + s) * heads + h
        return turned[:, first : first + 1]

    loads["state"].wait()
    readouts = []
    for s in range(seqs):
        rows = [
            jnp.sum(column(0, s, h) * state_v[s, h], axis=0, keepdims=True) for h in range(heads)
        ]
        match = jnp.sum(query[s] * key_part[s], axis=1, keepdims=True)
        readout = jnp.concatenate(rows, axis=0) + match * input_pre[s]
        mean_square = jnp.mean(readout * readout, axis=1, keepdims=True)
        readouts.append(readout * lax.rsqrt(mean_square + head_eps))
    loads["head_gain"].wait()
    outgate = projected(3)
    for s in range(seqs):
        gated_buf[s * heads : (s + 1) * heads, :] = (
            readouts[s] * head_gain_v[...] * jax.nn.silu(outgate[s])
        )
    gated = jnp.concatenate(
        [gated_buf[pl.ds(h, seqs, stride=heads), :] for h in range(heads)], axis=1
    ).astype(bf16)
    loads["out"].wait()
    step = per * lane
    for c in range(parts):
        part = jnp.dot(gated, out_v[:, c * step : (c + 1) * step], preferred_element_type=f32)
        for j in range(per):
            head_f32[c, pl.ds(j, seqs, stride=per), :] = part[:, j * lane : (j + 1) * lane]
        head_buf[c, tp] = head_f32[c].astype(bf16)
        for t in reversed(range(1, n_tp)):
            send(head_buf.at[c, tp], head_buf.at[c, tp], HEADS_SUM, head_sem.at[c], 0, t)

    for s in range(seqs):
        for h in range(heads):
            new_v[s, h] = (
                column(1, s, h) * state_v[s, h] + column(2, s, h) * input_pre[s][h : h + 1, :]
            )
    store = pltpu.make_async_copy(new_v, state_out, store_sem)
    store.start()

    streams = [[] for _ in range(seqs)]
    for c in range(parts):
        wait_for(head_sem.at[c], head_buf.at[c], n_tp - 1)
        head_total = tree_sum([head_buf[c, t].astype(f32) for t in range(n_tp)])
        for s in range(seqs):
            mixed_rows = residual[s][c] + head_total[s * per : (s + 1) * per]
            streams[s].append(mixed_rows.astype(bf16).astype(f32))
    norm_two = [norm_rows(streams[s], 1)[2] for s in range(seqs)]
    for c in range(parts):
        ag_two[c, kv] = jnp.concatenate([norm_two[s][c] for s in range(seqs)], axis=0)
        for k in reversed(range(1, n_kv)):
            send(ag_two.at[c, kv], ag_two.at[c, kv], AG_TWO, ag_sem.at[c], k, 0)

    wait_for(send_sem.at[RS_ONE], rs_recv_one, n - 1)
    loads["gate1"].wait()
    loads["up1"].wait()
    gate = up = None
    for c in range(parts):
        wait_for(ag_sem.at[c], ag_two.at[c], n_kv - 1)
        ag_two_f32[c] = ag_two[c].astype(f32).reshape(ag_two_f32.shape[1:])
        tiles = []
        for j in range(per):
            pieces = [
                ag_two_f32[c, pl.ds(s * per + j, n_kv, stride=part_rows), :] for s in range(seqs)
            ]
            tiles.append(jnp.concatenate(pieces, axis=0).astype(bf16))
            normed_bf[c * per + j] = tiles[-1]
        rows = jnp.concatenate(tiles, axis=1)
        cols = slice(c * step, (c + 1) * step)
        gate_part = dot_turned(rows, gate_v[1, :, cols])
        up_part = dot_turned(rows, up_v[1, :, cols])
        gate = gate_part if gate is None else gate + gate_part
        up = up_part if up is None else up + up_part
    reduce_scatter_start(hidden_of(gate, up), 1, RS_THREE, rs_recv_three)
    own_rows = residual_scale * normed_bf[me].astype(f32)

    row_ids = lax.broadcasted_iota(jnp.int32, (batch, lane), 0)
    lane_ids = lax.broadcasted_iota(jnp.int32, (batch, lane), 1)
    stream = own_rows + 0.5 * reduce_scatter_end(RS_THREE, rs_recv_three)
    own_mean = jnp.sum(stream, axis=1, keepdims=True) / lane
    own_centred = stream - own_mean
    own_spread = jnp.sum(own_centred * own_centred, axis=1, keepdims=True)

    def to_lanes(values):
        return jnp.sum(jnp.where(row_ids == lane_ids, values, 0.0), axis=0, keepdims=True)

    spread_buf[me] = jnp.concatenate([to_lanes(own_mean), to_lanes(own_spread)], axis=0)
    for k, t in peers:
        send(spread_buf.at[me], spread_buf.at[me], SPREAD, recv_sem.at[SPREAD], k, t)

    for s in range(seqs):
        final_buf[pl.ds(s, n_kv, stride=seqs), :] = stream[s * n_kv : (s + 1) * n_kv, :]
    natural = final_buf[...]
    for kind in (TOK, RS_THREE):
        wait_for(send_sem.at[kind], tok_buf, n - 1)
    wait_for(send_sem.at[GB], gb_buf, n - 1)
    wait_for(send_sem.at[TURN], turn_recv, n - 1)
    wait_for(send_sem.at[OWN_TP], own_tp, n_tp - 1)
    wait_for(send_sem.at[BASE], base_recv, n_kv - 1)
    for i in range(4):
        wait_for(send_sem.at[PROJ], proj_recv.at[i], n_kv - 1)
    for c in range(parts):
        wait_for(send_sem.at[HEADS_SUM], head_buf.at[c], n_tp - 1)
        wait_for(send_sem.at[AG_TWO], ag_two.at[c], n_kv - 1)
    store.wait()

    wait_for(recv_sem.at[SPREAD], spread_buf, n - 1)
    means = spread_buf[:, 0, :]
    mean_row = jnp.sum(means, axis=0, keepdims=True) / n
    apart = means - mean_row
    square_row = jnp.sum(spread_buf[:, 1, :] + lane * (apart * apart), axis=0, keepdims=True)
    scale_row = lax.rsqrt(square_row / width + norm_eps)
    place = lax.rem(row_ids, seqs) * n_kv + lax.div(row_ids, seqs)

    def to_rows(values):
        return jnp.sum(jnp.where(place == lane_ids, values, 0.0), axis=1, keepdims=True)

    mixed = (natural - to_rows(mean_row)) * to_rows(scale_row) * gains[2:3, :] + gains[5:6, :]
    mixed_ref[...] = mixed.astype(bf16)
    wait_for(send_sem.at[SPREAD], spread_buf, n - 1)


def fused(n_kv, n_tp, *args):
    (
        tokens,
        gate_weights,
        up_weights,
        down_weights,
        norm_gain,
        norm_bias,
        query_weight,
        forget_weight,
        input_weight,
        outgate_weight,
        lower_bound,
        head_gain,
        out_weight,
        state,
    ) = args
    batch, lane = tokens.shape
    n = n_kv * n_tp
    seqs, heads = state.shape[:2]
    gate_weights = jnp.swapaxes(gate_weights, 1, 2)
    up_weights = jnp.swapaxes(up_weights, 1, 2)
    bf16, f32 = jnp.bfloat16, jnp.float32
    per = 8
    parts, part_rows = n // per, per * seqs
    seq_rows = seqs * heads
    scratch = [
        pltpu.VMEM(gate_weights.shape, bf16),
        pltpu.VMEM(up_weights.shape, bf16),
        pltpu.VMEM(down_weights.shape, bf16),
        pltpu.VMEM((4, *query_weight.shape), bf16),
        pltpu.VMEM(out_weight.shape, bf16),
        pltpu.VMEM(state.shape, f32),
        pltpu.VMEM(state.shape, f32),
        pltpu.VMEM(norm_gain.shape, bf16),
        pltpu.VMEM(norm_bias.shape, bf16),
        pltpu.VMEM((heads, HEAD), f32),
        pltpu.VMEM((heads, HEAD), f32),
        pltpu.VMEM((n, batch, lane), bf16),
        pltpu.VMEM((n, 8, lane), f32),
        pltpu.VMEM((n, batch, lane), bf16),
        pltpu.VMEM((n, batch, lane), bf16),
        pltpu.VMEM((n, batch, lane), bf16),
        pltpu.VMEM((n_kv, seqs, lane), f32),
        pltpu.VMEM((n, seqs, lane), f32),
        pltpu.VMEM((n_tp, batch, lane), bf16),
        pltpu.VMEM((4, 2 * heads, HEAD), f32),
        pltpu.VMEM((4, 2 * heads, HEAD), bf16),
        pltpu.VMEM((n_kv, 4, 2 * heads, HEAD), bf16),
        pltpu.VMEM((4, batch * heads, HEAD), f32),
        pltpu.VMEM((4, n_kv, seq_rows, HEAD), bf16),
        pltpu.VMEM((4, n_kv, seq_rows, HEAD), bf16),
        pltpu.VMEM((seq_rows, HEAD), f32),
        pltpu.VMEM((parts, part_rows, lane), f32),
        pltpu.VMEM((parts, n_tp, part_rows, lane), bf16),
        pltpu.VMEM((parts, n_kv, part_rows, lane), bf16),
        pltpu.VMEM((parts, n_kv * part_rows, lane), f32),
        pltpu.VMEM((n, batch, lane), bf16),
        pltpu.VMEM((n, 2, lane), f32),
        pltpu.VMEM((batch, lane), f32),
        pltpu.SemaphoreType.DMA((len(KINDS) + 4,)),
        pltpu.SemaphoreType.DMA((len(KINDS),)),
        pltpu.SemaphoreType.DMA((n_kv,)),
        pltpu.SemaphoreType.DMA((4,)),
        pltpu.SemaphoreType.DMA((parts,)),
        pltpu.SemaphoreType.DMA((parts,)),
        pltpu.SemaphoreType.DMA((17,)),
        pltpu.SemaphoreType.DMA,
    ]
    vmem = pl.BlockSpec(memory_space=pltpu.VMEM)
    hbm = pl.BlockSpec(memory_space=pl.ANY)
    return pl.pallas_call(
        functools.partial(layer_kernel, n_kv, n_tp),
        out_shape=(
            jax.ShapeDtypeStruct(tokens.shape, bf16),
            jax.ShapeDtypeStruct(state.shape, f32),
        ),
        in_specs=[hbm] * 14,
        out_specs=(vmem, hbm),
        scratch_shapes=scratch,
        compiler_params=pltpu.CompilerParams(
            collective_id=0, has_side_effects=True, vmem_limit_bytes=60 * 1024 * 1024
        ),
        name="layer",
    )(
        tokens,
        norm_gain,
        norm_bias,
        lower_bound.reshape(heads, HEAD),
        head_gain.reshape(heads, HEAD),
        gate_weights,
        up_weights,
        down_weights,
        query_weight,
        forget_weight,
        input_weight,
        outgate_weight,
        out_weight,
        state,
    )


def power_of_two(count):
    return count & (count - 1) == 0


def dispatch(n_kv, n_tp, *args):
    tokens, state = args[0], args[13]
    batch, lane = tokens.shape
    seqs, heads = state.shape[:2]
    fits = lane == HEAD and batch == 16 and heads == 8 and seqs == 2 and n_kv == 8
    if fits and power_of_two(n_tp) and n_kv * n_tp % 8 == 0:
        return fused(n_kv, n_tp, *args)
    return local(*args)


def solution(mesh):
    n_kv, n_tp = mesh.shape["kv"], mesh.shape["tp"]
    return jax.shard_map(
        functools.partial(dispatch, n_kv, n_tp),
        mesh=mesh,
        in_specs=(
            P(None, ("kv", "tp")),
            P(None, None, ("kv", "tp")),
            P(None, None, ("kv", "tp")),
            P(None, ("kv", "tp"), None),
            P(None, ("kv", "tp")),
            P(None, ("kv", "tp")),
            P("kv", "tp"),
            P("kv", "tp"),
            P("kv", "tp"),
            P("kv", "tp"),
            P("tp"),
            P("tp"),
            P("tp", None),
            P("kv", "tp", None, None),
        ),
        out_specs=(P(None, ("kv", "tp")), P("kv", "tp", None, None)),
        check_vma=False,
    )
```

time: 62.9 us -> 53.5 us (0.85)
  Pallas kernels: 58.5 us -> 49.1 us
    pallas_call x1, Pallas kernels: 58.5 us -> 49.1 us  [fused(): pl.pallas_call(functools.partial(layer_kernel, n_kv, n_tp), out_shape=(ja...]
where the time goes in v1:
time: 53.5 us; the launch traced here: 53.3 us
  Pallas kernels  49.1 us (92%)
  local copies, waits for them, and re-layouts  3.57 us (7%)
  between operations  0.64 us (1%)
    pallas_call x1, Pallas kernels, fused(): pl.pallas_call(functools.partial(layer_kernel, n_kv, n_tp), out_shape=(ja...  49.1 us
    unnamed x2, local copies, waits for them, and re-layouts  3.57 us

profile of v1, /device:TPU:0, one launch (start us, length us, event | category | flops | bytes accessed | tf_op | source)
XLA Modules:
  0.0 53.3 jit_solution(9155351724817540802)
XLA Ops:
  0.6 49.1 %layer.1 = (bf16[16,128]{1,0:T(8,128)(2,1)}, f32[2,8,128,128]{3,2,1,0:T(8,128)}) custom-call(bf16[16,128]{1,0:T(8,128)(2,1)} %tokens_hbm.1, bf16[3,128]{1,0:T(4,128)(2,1)} %gain_hbm.1, bf16[3,128]{1,0:T(4,128)(2,1)} %bias_hbm.1, f32[8,128]{1,0:T(8,128)} %bitcast.6, f32[8,128]{1,0:T(8,128)} %bitcast.7, bf16[2,352,4096]{2,1,0:T(8,128)(2,1)} %bitcast.4, ...), custom_call_target="tpu_custom_call" | custom-call | tf_op jit(solution)/shard_map/layer/pallas_call | solution.py:613
  49.7 1.3 %copy.18 = bf16[16,128]{1,0:T(8,128)(2,1)} copy(bf16[16,128]{1,0:T(8,128)(2,1)} %get-tuple-element.4) | data formatting | bytes 8192
  51.0 2.3 %copy.19 = f32[2,8,128,128]{3,2,1,0:T(8,128)} copy(f32[2,8,128,128]{3,2,1,0:T(8,128)} %get-tuple-element.5) | data formatting | bytes 2097152

commit v2 on v1

--- a/solution.py
+++ b/solution.py
@@ -128,7 +128,7 @@
     return (mixed, updated)
 
 
-KINDS = ("gb", "rs_one", "turn", "own_tp", "base", "rs_three", "spread")
+KINDS = ("gain_tp", "gains", "rs_one", "turn", "turn_tp", "own_tp", "base", "bases", "rs_three", "spread")
 
 
 def tree_sum(terms):
@@ -176,29 +176,29 @@
     out_hbm,
     state_hbm,
     mixed_ref,
-    state_out,
+    new_v,
     gate_v,
     up_v,
     down_v,
     proj_v,
     out_v,
     state_v,
-    new_v,
     gain_v,
     bias_v,
     low_v,
     head_gain_v,
     tok_buf,
-    gb_buf,
+    gain_tp,
+    gain_buf,
     rs_send,
     rs_recv_one,
     rs_recv_three,
-    turn_send,
+    turn_tp,
     turn_recv,
     own_tp,
-    base_f32,
     base_send,
     base_recv,
+    base_all,
     proj_f32,
     proj_send,
     proj_recv,
@@ -217,7 +217,6 @@
     head_sem,
     ag_sem,
     load_sem,
-    store_sem,
 ):
     n = n_kv * n_tp
     batch, lane = tok_buf.shape[1:]
@@ -253,7 +252,8 @@
     order += [("down1", down_hbm.at[1], down_v.at[1])]
     for i, (name, source, target) in enumerate(order):
         loads[name] = pltpu.make_async_copy(source, target, load_sem.at[i])
-        loads[name].start()
+        if i < 10:
+            loads[name].start()
 
     def send(src, dst, kind, recv, k, t):
         pltpu.make_async_remote_copy(
@@ -269,20 +269,24 @@
         part = ref.at[pl.ds(0, count)]
         pltpu.make_async_copy(part, part, sem).wait()
 
-    GB, RS_ONE, TURN, OWN_TP, BASE, RS_THREE, SPREAD = range(len(KINDS))
+    GAIN_TP, GAINS, RS_ONE, TURN, TURN_TP, OWN_TP, BASE, BASES, RS_THREE, SPREAD = range(len(KINDS))
     TOK, PROJ, HEADS_SUM, AG_TWO = range(len(KINDS), len(KINDS) + 4)
 
     loads["gain"].wait()
     loads["bias"].wait()
     pad = jnp.zeros((2, lane), f32)
-    gains = jnp.concatenate([gain_v[...].astype(f32), bias_v[...].astype(f32), pad], axis=0)
-    gb_buf[me] = gains
+    gains, biases = gain_v[...].astype(f32), bias_v[...].astype(f32)
+    gains = jnp.concatenate([gains[0:2], biases[0:2], gains[2:3], biases[2:3], pad], axis=0)
+    gain_tp[tp] = gains
     loads["tokens"].wait()
     pl.semaphore_wait(barrier, n - 1)
     for k, t in peers:
         send(tok_buf.at[me], tok_buf.at[me], TOK, tok_sem.at[kv], k, t)
-    for k, t in peers:
-        send(gb_buf.at[me], gb_buf.at[me], GB, recv_sem.at[GB], k, t)
+    for t in reversed(range(1, n_tp)):
+        send(gain_tp.at[tp], gain_tp.at[tp], GAIN_TP, recv_sem.at[GAIN_TP], 0, t)
+
+    for name in [entry[0] for entry in order[10:]]:
+        loads[name].start()
 
     def columns(index, size):
         return pl.ds(pl.multiple_of(index * size, size), size)
@@ -309,9 +313,31 @@
         wait_for(recv_sem.at[kind], recv, n - 1)
         return tree_sum([recv[j].astype(f32) for j in range(n)])
 
+    def send_bases():
+        wait_for(recv_sem.at[GAIN_TP], gain_tp, n_tp - 1)
+        for t in range(n_tp):
+            gain_buf[kv * n_tp + t] = gain_tp[t, 0:4]
+        own_gains = gain_tp.at[:, pl.ds(0, 4)]
+        for k in reversed(range(1, n_kv)):
+            target = gain_buf.at[pl.ds(kv * n_tp, n_tp)]
+            send(own_gains, target, GAINS, recv_sem.at[GAINS], k, 0)
+        kv_gains = jnp.concatenate([gain_tp[t] for t in range(n_tp)], axis=1).astype(bf16)
+        for i in range(4):
+            loads["proj%d" % i].wait()
+            based = jnp.dot(kv_gains, proj_v[i], preferred_element_type=f32)
+            for h in range(heads):
+                block = slice(h * HEAD, (h + 1) * HEAD)
+                base_send[2 * i, h : h + 1, :] = based[0:1, block]
+                base_send[2 * i + 1, h : h + 1, :] = based[2:3, block]
+        for k in reversed(range(1, n_kv)):
+            send(base_send.at[kv_of[k]], base_recv.at[kv], BASE, recv_sem.at[BASE], k, 0)
+        base_recv[kv] = base_send[kv]
+
     gate = up = None
     for k in range(n_kv):
         source = kv_of[k]
+        if k == n_kv // 2:
+            send_bases()
         wait_for(tok_sem.at[source], tok_buf, n_tp if k else n_tp - 1)
         rows = jnp.concatenate([tok_buf[source * n_tp + t] for t in range(n_tp)], axis=1)
         cols = columns(source, group)
@@ -330,32 +356,27 @@
     centre = residual_scale * token_sum / width
     own_tokens = residual_scale * tok_buf[me].astype(f32) - centre
 
-    wait_for(recv_sem.at[GB], gb_buf, n - 1)
-    kv_gains = jnp.concatenate([gb_buf[kv * n_tp + t] for t in range(n_tp)], axis=1).astype(bf16)
-    for i in range(4):
-        loads["proj%d" % i].wait()
-        based = jnp.dot(kv_gains, proj_v[i], preferred_element_type=f32)
-        for h in range(heads):
-            block = slice(h * HEAD, (h + 1) * HEAD)
-            base_f32[i, h : h + 1, :] = based[0:1, block]
-            base_f32[i, heads + h : heads + h + 1, :] = based[3:4, block]
-    base_send[...] = base_f32[...].astype(bf16)
+    wait_for(recv_sem.at[BASE], base_recv, n_kv - 1)
+    base_all[kv] = tree_sum([base_recv[j] for j in range(n_kv)])
     for k in reversed(range(1, n_kv)):
-        send(base_send, base_recv.at[kv], BASE, recv_sem.at[BASE], k, 0)
-    base_recv[kv] = base_send[...]
-
+        send(base_all.at[kv], base_all.at[kv], BASES, recv_sem.at[BASES], k, 0)
     shifted = own_tokens + 0.5 * reduce_scatter_end(RS_ONE, rs_recv_one)
     own_tp[tp] = (shifted * gains[0:1, :]).astype(bf16)
     for t in reversed(range(1, n_tp)):
         send(own_tp.at[tp], own_tp.at[tp], OWN_TP, recv_sem.at[OWN_TP], 0, t)
     for j in range(n_kv):
-        turn_send[j] = shifted[j * seqs : (j + 1) * seqs, :]
-    for k, t in peers:
-        send(turn_send.at[kv_of[k]], turn_recv.at[me], TURN, recv_sem.at[TURN], k, t)
-    turn_recv[me] = turn_send[kv]
+        turn_tp[tp, j] = shifted[j * seqs : (j + 1) * seqs, :]
+    for t in reversed(range(1, n_tp)):
+        send(turn_tp.at[tp], turn_tp.at[tp], TURN_TP, recv_sem.at[TURN_TP], 0, t)
 
     wait_for(recv_sem.at[OWN_TP], own_tp, n_tp - 1)
     block = jnp.concatenate([own_tp[t] for t in range(n_tp)], axis=1)
+    wait_for(recv_sem.at[TURN_TP], turn_tp, n_tp - 1)
+    own_turn = turn_recv.at[pl.ds(kv * n_tp, n_tp)]
+    for k in reversed(range(1, n_kv)):
+        send(turn_tp.at[:, kv_of[k]], own_turn, TURN, recv_sem.at[TURN], k, 0)
+    for t in range(n_tp):
+        turn_recv[kv * n_tp + t] = turn_tp[t, kv]
     turns = (1, 2, 0, 3)
     for i in turns:
         part = jnp.dot(block, proj_v[i], preferred_element_type=f32)
@@ -369,30 +390,28 @@
             send(proj_send.at[i, kv_of[k]], proj_recv.at[i, kv], PROJ, proj_sem.at[i], k, 0)
         proj_recv[i, kv] = proj_send[i, kv]
 
-    wait_for(recv_sem.at[BASE], base_recv, n_kv - 1)
-    base = tree_sum([base_recv[j].astype(f32) for j in range(n_kv)])
-    wait_for(recv_sem.at[TURN], turn_recv, n - 1)
-
-    def gain_rows(c, index):
-        return gb_buf[c * per : (c + 1) * per, index, :]
-
-    def norm_rows(tiles, index):
+    wait_for(recv_sem.at[TURN], turn_recv, n - n_tp)
+
+    def norm_stats(tiles):
         mean = total_of(tiles) / width
         centred = [tile - mean for tile in tiles]
         scale = lax.rsqrt(total_of([c * c for c in centred]) / width + norm_eps)
-        normed = [
-            (tile * scale * gain_rows(c, index) + gain_rows(c, 3 + index)).astype(bf16)
-            for c, tile in enumerate(centred)
+        return mean, scale, centred
+
+    def normed_rows(stats, index):
+        return [
+            (
+                tile * stats[1] * gain_buf[c * per : (c + 1) * per, index, :]
+                + gain_buf[c * per : (c + 1) * per, 2 + index, :]
+            ).astype(bf16)
+            for c, tile in enumerate(stats[2])
         ]
-        return mean, scale, normed
 
     norm_one = [
-        norm_rows([turn_recv[c * per : (c + 1) * per, s, :] for c in range(parts)], 0)
+        norm_stats([turn_recv[c * per : (c + 1) * per, s, :] for c in range(parts)])
         for s in range(seqs)
     ]
-    residual = [
-        [residual_scale * tile.astype(f32) for tile in norm_one[s][2]] for s in range(seqs)
-    ]
+    wait_for(recv_sem.at[BASES], base_all, n_kv - 1)
 
     def projected(i):
         wait_for(proj_sem.at[i], proj_recv.at[i], n_kv - 1)
@@ -400,8 +419,8 @@
         found = []
         for s in range(seqs):
             mean, scale, _ = norm_one[s]
-            rows = total[s * heads : (s + 1) * heads] - mean * base[i, 0:heads]
-            rows = scale * rows + base[i, heads : 2 * heads]
+            rows = total[s * heads : (s + 1) * heads] - mean * base_all[2 * i]
+            rows = scale * rows + base_all[2 * i + 1]
             found.append(rows.astype(bf16).astype(f32))
         return found
 
@@ -454,9 +473,12 @@
             new_v[s, h] = (
                 column(1, s, h) * state_v[s, h] + column(2, s, h) * input_pre[s][h : h + 1, :]
             )
-    store = pltpu.make_async_copy(new_v, state_out, store_sem)
-    store.start()
-
+
+    wait_for(recv_sem.at[GAINS], gain_buf, n - n_tp)
+    residual = [
+        [residual_scale * tile.astype(f32) for tile in normed_rows(norm_one[s], 0)]
+        for s in range(seqs)
+    ]
     streams = [[] for _ in range(seqs)]
     for c in range(parts):
         wait_for(head_sem.at[c], head_buf.at[c], n_tp - 1)
@@ -464,7 +486,7 @@
         for s in range(seqs):
             mixed_rows = residual[s][c] + head_total[s * per : (s + 1) * per]
             streams[s].append(mixed_rows.astype(bf16).astype(f32))
-    norm_two = [norm_rows(streams[s], 1)[2] for s in range(seqs)]
+    norm_two = [normed_rows(norm_stats(streams[s]), 1) for s in range(seqs)]
     for c in range(parts):
         ag_two[c, kv] = jnp.concatenate([norm_two[s][c] for s in range(seqs)], axis=0)
         for k in reversed(range(1, n_kv)):
@@ -512,16 +534,18 @@
     natural = final_buf[...]
     for kind in (TOK, RS_THREE):
         wait_for(send_sem.at[kind], tok_buf, n - 1)
-    wait_for(send_sem.at[GB], gb_buf, n - 1)
-    wait_for(send_sem.at[TURN], turn_recv, n - 1)
+    wait_for(send_sem.at[GAINS], gain_buf, n - n_tp)
+    wait_for(send_sem.at[TURN_TP], turn_tp, n_tp - 1)
+    wait_for(send_sem.at[GAIN_TP], gain_tp, n_tp - 1)
+    wait_for(send_sem.at[TURN], turn_recv, n - n_tp)
     wait_for(send_sem.at[OWN_TP], own_tp, n_tp - 1)
     wait_for(send_sem.at[BASE], base_recv, n_kv - 1)
+    wait_for(send_sem.at[BASES], base_all, n_kv - 1)
     for i in range(4):
         wait_for(send_sem.at[PROJ], proj_recv.at[i], n_kv - 1)
     for c in range(parts):
         wait_for(send_sem.at[HEADS_SUM], head_buf.at[c], n_tp - 1)
         wait_for(send_sem.at[AG_TWO], ag_two.at[c], n_kv - 1)
-    store.wait()
 
     wait_for(recv_sem.at[SPREAD], spread_buf, n - 1)
     means = spread_buf[:, 0, :]
@@ -534,9 +558,20 @@
     def to_rows(values):
         return jnp.sum(jnp.where(place == lane_ids, values, 0.0), axis=1, keepdims=True)
 
-    mixed = (natural - to_rows(mean_row)) * to_rows(scale_row) * gains[2:3, :] + gains[5:6, :]
+    mixed = (natural - to_rows(mean_row)) * to_rows(scale_row) * gains[4:5, :] + gains[5:6, :]
     mixed_ref[...] = mixed.astype(bf16)
     wait_for(send_sem.at[SPREAD], spread_buf, n - 1)
+
+
+def store_kernel(mixed_v, new_v, mixed_out, state_out, sem):
+    copies = [
+        pltpu.make_async_copy(new_v, state_out, sem.at[0]),
+        pltpu.make_async_copy(mixed_v, mixed_out, sem.at[1]),
+    ]
+    for copy in copies:
+        copy.start()
+    for copy in copies:
+        copy.wait()
 
 
 def fused(n_kv, n_tp, *args):
@@ -572,22 +607,22 @@
         pltpu.VMEM((4, *query_weight.shape), bf16),
         pltpu.VMEM(out_weight.shape, bf16),
         pltpu.VMEM(state.shape, f32),
-        pltpu.VMEM(state.shape, f32),
         pltpu.VMEM(norm_gain.shape, bf16),
         pltpu.VMEM(norm_bias.shape, bf16),
         pltpu.VMEM((heads, HEAD), f32),
         pltpu.VMEM((heads, HEAD), f32),
         pltpu.VMEM((n, batch, lane), bf16),
-        pltpu.VMEM((n, 8, lane), f32),
+        pltpu.VMEM((n_tp, 8, lane), f32),
+        pltpu.VMEM((n, 4, lane), f32),
         pltpu.VMEM((n, batch, lane), bf16),
         pltpu.VMEM((n, batch, lane), bf16),
         pltpu.VMEM((n, batch, lane), bf16),
-        pltpu.VMEM((n_kv, seqs, lane), f32),
+        pltpu.VMEM((n_tp, n_kv, seqs, lane), f32),
         pltpu.VMEM((n, seqs, lane), f32),
         pltpu.VMEM((n_tp, batch, lane), bf16),
-        pltpu.VMEM((4, 2 * heads, HEAD), f32),
-        pltpu.VMEM((4, 2 * heads, HEAD), bf16),
-        pltpu.VMEM((n_kv, 4, 2 * heads, HEAD), bf16),
+        pltpu.VMEM((n_kv, heads, HEAD), f32),
+        pltpu.VMEM((n_kv, heads, HEAD), f32),
+        pltpu.VMEM((n_kv, heads, HEAD), f32),
         pltpu.VMEM((4, batch * heads, HEAD), f32),
         pltpu.VMEM((4, n_kv, seq_rows, HEAD), bf16),
         pltpu.VMEM((4, n_kv, seq_rows, HEAD), bf16),
@@ -606,24 +641,20 @@
         pltpu.SemaphoreType.DMA((parts,)),
         pltpu.SemaphoreType.DMA((parts,)),
         pltpu.SemaphoreType.DMA((17,)),
-        pltpu.SemaphoreType.DMA,
     ]
     vmem = pl.BlockSpec(memory_space=pltpu.VMEM)
     hbm = pl.BlockSpec(memory_space=pl.ANY)
-    return pl.pallas_call(
+    held = pl.pallas_call(
         functools.partial(layer_kernel, n_kv, n_tp),
-        out_shape=(
-            jax.ShapeDtypeStruct(tokens.shape, bf16),
-            jax.ShapeDtypeStruct(state.shape, f32),
-        ),
+        out_shape=(pltpu.VMEM(tokens.shape, bf16), pltpu.VMEM(state.shape, f32)),
         in_specs=[hbm] * 14,
-        out_specs=(vmem, hbm),
+        out_specs=(vmem, vmem),
         scratch_shapes=scratch,
         compiler_params=pltpu.CompilerParams(
-            collective_id=0, has_side_effects=True, vmem_limit_bytes=60 * 1024 * 1024
+            collective_id=0, has_side_effects=True, vmem_limit_bytes=44 * 1024 * 1024
         ),
         name="layer",
-    )(
+    )(*[pltpu.with_memory_space_constraint(operand, pltpu.HBM) for operand in (
         tokens,
         norm_gain,
         norm_bias,
@@ -638,7 +669,19 @@
         outgate_weight,
         out_weight,
         state,
-    )
+    )])
+    return pl.pallas_call(
+        store_kernel,
+        out_shape=(
+            jax.ShapeDtypeStruct(tokens.shape, bf16),
+            jax.ShapeDtypeStruct(state.shape, f32),
+        ),
+        in_specs=[vmem, vmem],
+        out_specs=(hbm, hbm),
+        scratch_shapes=[pltpu.SemaphoreType.DMA((2,))],
+        compiler_params=pltpu.CompilerParams(vmem_limit_bytes=4 * 1024 * 1024),
+        name="store",
+    )(*held)
 
 
 def power_of_two(count):

time: 53.5 us -> 50.2 us (0.938)
  local copies, waits for them, and re-layouts: 3.57 us -> 0 us
    unnamed x2 -> x0, local copies, waits for them, and re-layouts: 3.57 us -> none
    pallas_call x1 -> x2, Pallas kernels: 49.1 us -> 49.4 us  [the longest x1 48.4 us: fused(): pl.pallas_call(functools.partial(layer_kernel, n_kv, n_tp), out_shape=(pl...]
where the time goes in v2:
time: 50.2 us; the launch traced here: 50 us
  Pallas kernels  49.4 us (98%)
  between operations  0.64 us (1%)
    pallas_call x1, Pallas kernels, fused(): pl.pallas_call(functools.partial(layer_kernel, n_kv, n_tp), out_shape=(pl...  48.4 us

profile of v2, /device:TPU:0, one launch (start us, length us, event | category | flops | bytes accessed | tf_op | source)
XLA Modules:
  0.0 50.0 jit_solution(15114776090904095986)
XLA Ops:
  0.6 48.4 %layer.1 = (bf16[16,128]{1,0:T(8,128)(2,1)S(1)}, f32[2,8,128,128]{3,2,1,0:T(8,128)S(1)}) custom-call(bf16[16,128]{1,0:T(8,128)(2,1)} %tokens_hbm.1, bf16[3,128]{1,0:T(4,128)(2,1)} %gain_hbm.1, bf16[3,128]{1,0:T(4,128)(2,1)} %bias_hbm.1, f32[8,128]{1,0:T(8,128)} %bitcast.6, f32[8,128]{1,0:T(8,128)} %bitcast.7, bf16[2,352,4096]{2,1,0:T(8,128)(2,1)} %bitcast.4, ...), custom_call_target="tpu_custom_call" | custom-call | tf_op jit(solution)/shard_map/layer/pallas_call | solution.py:647
  49.0 1.0 %store.1 = (bf16[16,128]{1,0:T(8,128)(2,1)}, f32[2,8,128,128]{3,2,1,0:T(8,128)}) custom-call(bf16[16,128]{1,0:T(8,128)(2,1)S(1)} %get-tuple-element.4.mixed_v, f32[2,8,128,128]{3,2,1,0:T(8,128)S(1)} %get-tuple-element.5.new_v), custom_call_target="tpu_custom_call" | custom-call | tf_op jit(solution)/shard_map/store/pallas_call | solution.py:673

commit v3 on v2

--- a/solution.py
+++ b/solution.py
@@ -128,7 +128,7 @@
     return (mixed, updated)
 
 
-KINDS = ("gain_tp", "gains", "rs_one", "turn", "turn_tp", "own_tp", "base", "bases", "rs_three", "spread")
+KINDS = ("gain_tp", "gains", "rs_one", "turn", "turn_tp", "own_tp", "base", "bases", "stat_two", "rs_three", "spread")
 
 
 def tree_sum(terms):
@@ -179,6 +179,8 @@
     new_v,
     gate_v,
     up_v,
+    gate_t,
+    up_t,
     down_v,
     proj_v,
     out_v,
@@ -207,6 +209,7 @@
     head_buf,
     ag_two,
     ag_two_f32,
+    stat_two,
     normed_bf,
     spread_buf,
     final_buf,
@@ -269,7 +272,7 @@
         part = ref.at[pl.ds(0, count)]
         pltpu.make_async_copy(part, part, sem).wait()
 
-    GAIN_TP, GAINS, RS_ONE, TURN, TURN_TP, OWN_TP, BASE, BASES, RS_THREE, SPREAD = range(len(KINDS))
+    GAIN_TP, GAINS, RS_ONE, TURN, TURN_TP, OWN_TP, BASE, BASES, STAT_TWO, RS_THREE, SPREAD = range(len(KINDS))
     TOK, PROJ, HEADS_SUM, AG_TWO = range(len(KINDS), len(KINDS) + 4)
 
     loads["gain"].wait()
@@ -312,6 +315,16 @@
     def reduce_scatter_end(kind, recv):
         wait_for(recv_sem.at[kind], recv, n - 1)
         return tree_sum([recv[j].astype(f32) for j in range(n)])
+
+    def turn_weights(layer):
+        loads["gate%d" % layer].wait()
+        loads["up%d" % layer].wait()
+        for source, target in ((gate_v, gate_t), (up_v, up_t)):
+
+            @pl.loop(0, width // (2 * lane))
+            def _(i):
+                rows = columns(i, 2 * lane)
+                target[layer, rows, :] = source[layer, :, rows].T
 
     def send_bases():
         wait_for(recv_sem.at[GAIN_TP], gain_tp, n_tp - 1)
@@ -333,33 +346,27 @@
             send(base_send.at[kv_of[k]], base_recv.at[kv], BASE, recv_sem.at[BASE], k, 0)
         base_recv[kv] = base_send[kv]
 
+    turn_weights(0)
     gate = up = None
     for k in range(n_kv):
         source = kv_of[k]
-        if k == n_kv // 2:
-            send_bases()
         wait_for(tok_sem.at[source], tok_buf, n_tp if k else n_tp - 1)
         rows = jnp.concatenate([tok_buf[source * n_tp + t] for t in range(n_tp)], axis=1)
         cols = columns(source, group)
-        if k == 0:
-            loads["gate0"].wait()
-            loads["up0"].wait()
-        gate_part = dot_turned(rows, gate_v[0, :, cols])
-        up_part = dot_turned(rows, up_v[0, :, cols])
+        gate_part = jnp.dot(rows, gate_t[0, cols, :], preferred_element_type=f32)
+        up_part = jnp.dot(rows, up_t[0, cols, :], preferred_element_type=f32)
         gate = gate_part if gate is None else gate + gate_part
         up = up_part if up is None else up + up_part
     reduce_scatter_start(hidden_of(gate, up), 0, RS_ONE, rs_recv_one)
 
+    send_bases()
+    turn_weights(1)
     token_sum = jnp.sum(
         tree_sum([tok_buf[j].astype(f32) for j in range(n)]), axis=1, keepdims=True
     )
     centre = residual_scale * token_sum / width
     own_tokens = residual_scale * tok_buf[me].astype(f32) - centre
 
-    wait_for(recv_sem.at[BASE], base_recv, n_kv - 1)
-    base_all[kv] = tree_sum([base_recv[j] for j in range(n_kv)])
-    for k in reversed(range(1, n_kv)):
-        send(base_all.at[kv], base_all.at[kv], BASES, recv_sem.at[BASES], k, 0)
     shifted = own_tokens + 0.5 * reduce_scatter_end(RS_ONE, rs_recv_one)
     own_tp[tp] = (shifted * gains[0:1, :]).astype(bf16)
     for t in reversed(range(1, n_tp)):
@@ -369,6 +376,10 @@
     for t in reversed(range(1, n_tp)):
         send(turn_tp.at[tp], turn_tp.at[tp], TURN_TP, recv_sem.at[TURN_TP], 0, t)
 
+    wait_for(recv_sem.at[BASE], base_recv, n_kv - 1)
+    base_all[kv] = tree_sum([base_recv[j] for j in range(n_kv)])
+    for k in reversed(range(1, n_kv)):
+        send(base_all.at[kv], base_all.at[kv], BASES, recv_sem.at[BASES], k, 0)
     wait_for(recv_sem.at[OWN_TP], own_tp, n_tp - 1)
     block = jnp.concatenate([own_tp[t] for t in range(n_tp)], axis=1)
     wait_for(recv_sem.at[TURN_TP], turn_tp, n_tp - 1)
@@ -390,6 +401,10 @@
             send(proj_send.at[i, kv_of[k]], proj_recv.at[i, kv], PROJ, proj_sem.at[i], k, 0)
         proj_recv[i, kv] = proj_send[i, kv]
 
+    wait_for(recv_sem.at[GAINS], gain_buf, n - n_tp)
+    all_gains = jnp.concatenate([gain_buf[j] for j in range(n)], axis=1).astype(bf16)
+    gate_fixed = jnp.dot(all_gains, gate_t[1], preferred_element_type=f32)
+    up_fixed = jnp.dot(all_gains, up_t[1], preferred_element_type=f32)
     wait_for(recv_sem.at[TURN], turn_recv, n - n_tp)
 
     def norm_stats(tiles):
@@ -474,27 +489,33 @@
                 column(1, s, h) * state_v[s, h] + column(2, s, h) * input_pre[s][h : h + 1, :]
             )
 
-    wait_for(recv_sem.at[GAINS], gain_buf, n - n_tp)
     residual = [
         [residual_scale * tile.astype(f32) for tile in normed_rows(norm_one[s], 0)]
         for s in range(seqs)
     ]
+    middle = [total_of(residual[s]) / width for s in range(seqs)]
     streams = [[] for _ in range(seqs)]
     for c in range(parts):
         wait_for(head_sem.at[c], head_buf.at[c], n_tp - 1)
         head_total = tree_sum([head_buf[c, t].astype(f32) for t in range(n_tp)])
         for s in range(seqs):
             mixed_rows = residual[s][c] + head_total[s * per : (s + 1) * per]
-            streams[s].append(mixed_rows.astype(bf16).astype(f32))
-    norm_two = [normed_rows(norm_stats(streams[s]), 1) for s in range(seqs)]
-    for c in range(parts):
-        ag_two[c, kv] = jnp.concatenate([norm_two[s][c] for s in range(seqs)], axis=0)
+            streams[s].append(mixed_rows.astype(bf16).astype(f32) - middle[s])
+        gain_rows = gain_buf[c * per : (c + 1) * per, 1, :]
+        ag_two[c, kv] = jnp.concatenate(
+            [streams[s][c] * gain_rows for s in range(seqs)], axis=0
+        ).astype(bf16)
         for k in reversed(range(1, n_kv)):
             send(ag_two.at[c, kv], ag_two.at[c, kv], AG_TWO, ag_sem.at[c], k, 0)
+    stats = [norm_stats(streams[s]) for s in range(seqs)]
+    for i in range(2):
+        for s in range(seqs):
+            row = jnp.broadcast_to(stats[s][i], (1, lane))
+            stat_two[kv, i * seqs + s : i * seqs + s + 1, :] = row
+    for k in reversed(range(1, n_kv)):
+        send(stat_two.at[kv], stat_two.at[kv], STAT_TWO, recv_sem.at[STAT_TWO], k, 0)
 
     wait_for(send_sem.at[RS_ONE], rs_recv_one, n - 1)
-    loads["gate1"].wait()
-    loads["up1"].wait()
     gate = up = None
     for c in range(parts):
         wait_for(ag_sem.at[c], ag_two.at[c], n_kv - 1)
@@ -508,12 +529,20 @@
             normed_bf[c * per + j] = tiles[-1]
         rows = jnp.concatenate(tiles, axis=1)
         cols = slice(c * step, (c + 1) * step)
-        gate_part = dot_turned(rows, gate_v[1, :, cols])
-        up_part = dot_turned(rows, up_v[1, :, cols])
+        gate_part = jnp.dot(rows, gate_t[1, cols, :], preferred_element_type=f32)
+        up_part = jnp.dot(rows, up_t[1, cols, :], preferred_element_type=f32)
         gate = gate_part if gate is None else gate + gate_part
         up = up_part if up is None else up + up_part
+    wait_for(recv_sem.at[STAT_TWO], stat_two, n_kv - 1)
+    mean_two, scale_two = [
+        jnp.concatenate([stat_two[:, i * seqs + s, :] for s in range(seqs)], axis=0)[:, 0:1]
+        for i in range(2)
+    ]
+    gate = scale_two * (gate - mean_two * gate_fixed[1:2]) + gate_fixed[3:4]
+    up = scale_two * (up - mean_two * up_fixed[1:2]) + up_fixed[3:4]
     reduce_scatter_start(hidden_of(gate, up), 1, RS_THREE, rs_recv_three)
-    own_rows = residual_scale * normed_bf[me].astype(f32)
+    own_rows = scale_two * (normed_bf[me].astype(f32) - mean_two * gains[1:2]) + gains[3:4]
+    own_rows = residual_scale * own_rows
 
     row_ids = lax.broadcasted_iota(jnp.int32, (batch, lane), 0)
     lane_ids = lax.broadcasted_iota(jnp.int32, (batch, lane), 1)
@@ -543,6 +572,7 @@
     wait_for(send_sem.at[BASES], base_all, n_kv - 1)
     for i in range(4):
         wait_for(send_sem.at[PROJ], proj_recv.at[i], n_kv - 1)
+    wait_for(send_sem.at[STAT_TWO], stat_two, n_kv - 1)
     for c in range(parts):
         wait_for(send_sem.at[HEADS_SUM], head_buf.at[c], n_tp - 1)
         wait_for(send_sem.at[AG_TWO], ag_two.at[c], n_kv - 1)
@@ -603,6 +633,8 @@
     scratch = [
         pltpu.VMEM(gate_weights.shape, bf16),
         pltpu.VMEM(up_weights.shape, bf16),
+        pltpu.VMEM((2, n * lane, gate_weights.shape[1]), bf16),
+        pltpu.VMEM((2, n * lane, gate_weights.shape[1]), bf16),
         pltpu.VMEM(down_weights.shape, bf16),
         pltpu.VMEM((4, *query_weight.shape), bf16),
         pltpu.VMEM(out_weight.shape, bf16),
@@ -631,6 +663,7 @@
         pltpu.VMEM((parts, n_tp, part_rows, lane), bf16),
         pltpu.VMEM((parts, n_kv, part_rows, lane), bf16),
         pltpu.VMEM((parts, n_kv * part_rows, lane), f32),
+        pltpu.VMEM((n_kv, 2 * seqs, lane), f32),
         pltpu.VMEM((n, batch, lane), bf16),
         pltpu.VMEM((n, 2, lane), f32),
         pltpu.VMEM((batch, lane), f32),
@@ -651,7 +684,7 @@
         out_specs=(vmem, vmem),
         scratch_shapes=scratch,
         compiler_params=pltpu.CompilerParams(
-            collective_id=0, has_side_effects=True, vmem_limit_bytes=44 * 1024 * 1024
+            collective_id=0, has_side_effects=True, vmem_limit_bytes=58 * 1024 * 1024
         ),
         name="layer",
     )(*[pltpu.with_memory_space_constraint(operand, pltpu.HBM) for operand in (

time: 50.2 us -> 49 us (0.976)
  Pallas kernels: 49.4 us -> 48.1 us
    pallas_call x1, Pallas kernels: 48.4 us -> 47.2 us  [fused(): pl.pallas_call(functools.partial(layer_kernel, n_kv, n_tp), out_shape=(pl...]
where the time goes in v3:
time: 49 us; the launch traced here: 48.8 us
  Pallas kernels  48.1 us (98%)
  between operations  0.64 us (1%)
    pallas_call x1, Pallas kernels, fused(): pl.pallas_call(functools.partial(layer_kernel, n_kv, n_tp), out_shape=(pl...  47.2 us
    pallas_call x1, Pallas kernels, fused(): pl.pallas_call(store_kernel, out_shape=(jax.ShapeDtypeStruct(tokens.shape...  0.99 us

profile of v3, /device:TPU:0, one launch (start us, length us, event | category | flops | bytes accessed | tf_op | source)
XLA Modules:
  0.0 48.8 jit_solution(15148108113231218410)
XLA Ops:
  0.6 47.2 %layer.1 = (bf16[16,128]{1,0:T(8,128)(2,1)S(1)}, f32[2,8,128,128]{3,2,1,0:T(8,128)S(1)}) custom-call(bf16[16,128]{1,0:T(8,128)(2,1)} %tokens_hbm.1, bf16[3,128]{1,0:T(4,128)(2,1)} %gain_hbm.1, bf16[3,128]{1,0:T(4,128)(2,1)} %bias_hbm.1, f32[8,128]{1,0:T(8,128)} %bitcast.6, f32[8,128]{1,0:T(8,128)} %bitcast.7, bf16[2,352,4096]{2,1,0:T(8,128)(2,1)} %bitcast.4, ...), custom_call_target="tpu_custom_call" | custom-call | tf_op jit(solution)/shard_map/layer/pallas_call | solution.py:680
  47.8 1.0 %store.1 = (bf16[16,128]{1,0:T(8,128)(2,1)}, f32[2,8,128,128]{3,2,1,0:T(8,128)}) custom-call(bf16[16,128]{1,0:T(8,128)(2,1)S(1)} %get-tuple-element.4.mixed_v, f32[2,8,128,128]{3,2,1,0:T(8,128)S(1)} %get-tuple-element.5.new_v), custom_call_target="tpu_custom_call" | custom-call | tf_op jit(solution)/shard_map/store/pallas_call | solution.py:706

commit v4 on v3

--- a/solution.py
+++ b/solution.py
@@ -348,11 +348,15 @@
 
     turn_weights(0)
     gate = up = None
-    for k in range(n_kv):
-        source = kv_of[k]
-        wait_for(tok_sem.at[source], tok_buf, n_tp if k else n_tp - 1)
-        rows = jnp.concatenate([tok_buf[source * n_tp + t] for t in range(n_tp)], axis=1)
-        cols = columns(source, group)
+    for k in range(0, n_kv, 2):
+        sources = (kv_of[k], kv_of[k + 1])
+        for i, source in enumerate(sources):
+            wait_for(tok_sem.at[source], tok_buf, n_tp if k + i else n_tp - 1)
+        low_group = lax.div(kv_of[k], 2)
+        rows = jnp.concatenate(
+            [tok_buf[low_group * 2 * n_tp + t] for t in range(2 * n_tp)], axis=1
+        )
+        cols = columns(low_group, 2 * group)
         gate_part = jnp.dot(rows, gate_t[0, cols, :], preferred_element_type=f32)
         up_part = jnp.dot(rows, up_t[0, cols, :], preferred_element_type=f32)
         gate = gate_part if gate is None else gate + gate_part

time: 49 us -> 48.8 us (level)
  no operation moved by 1% of the time
where the time goes in v4:
time: 48.8 us; the launch traced here: 48.7 us
  Pallas kernels  48 us (98%)
  between operations  0.64 us (1%)
    pallas_call x1, Pallas kernels, fused(): pl.pallas_call(functools.partial(layer_kernel, n_kv, n_tp), out_shape=(pl...  47 us
    pallas_call x1, Pallas kernels, fused(): pl.pallas_call(store_kernel, out_shape=(jax.ShapeDtypeStruct(tokens.shape...  0.99 us

profile of v4, /device:TPU:0, one launch (start us, length us, event | category | flops | bytes accessed | tf_op | source)
XLA Modules:
  0.0 48.7 jit_solution(5566842591185927093)
XLA Ops:
  0.6 47.0 %layer.1 = (bf16[16,128]{1,0:T(8,128)(2,1)S(1)}, f32[2,8,128,128]{3,2,1,0:T(8,128)S(1)}) custom-call(bf16[16,128]{1,0:T(8,128)(2,1)} %tokens_hbm.1, bf16[3,128]{1,0:T(4,128)(2,1)} %gain_hbm.1, bf16[3,128]{1,0:T(4,128)(2,1)} %bias_hbm.1, f32[8,128]{1,0:T(8,128)} %bitcast.6, f32[8,128]{1,0:T(8,128)} %bitcast.7, bf16[2,352,4096]{2,1,0:T(8,128)(2,1)} %bitcast.4, ...), custom_call_target="tpu_custom_call" | custom-call | tf_op jit(solution)/shard_map/layer/pallas_call | solution.py:684
  47.7 1.0 %store.1 = (bf16[16,128]{1,0:T(8,128)(2,1)}, f32[2,8,128,128]{3,2,1,0:T(8,128)}) custom-call(bf16[16,128]{1,0:T(8,128)(2,1)S(1)} %get-tuple-element.4.mixed_v, f32[2,8,128,128]{3,2,1,0:T(8,128)S(1)} %get-tuple-element.5.new_v), custom_call_target="tpu_custom_call" | custom-call | tf_op jit(solution)/shard_map/store/pallas_call | solution.py:710
